TPU v7x, 256 devices: a whole 4x4x8 slice. The times are simulated.
256 devices in a mesh: sp: 32 (over z, x), tp: 8 (over y, core).
Axes of the slice: x: 4, y: 4, z: 8, core: 2. Of those that a mesh axis runs over, the one named last changes fastest.
Arguments:
- tokens: bfloat16 [16384, 2048], P(('sp', 'tp')), may hold values from -40 to 40
- query_weight: bfloat16 [2048, 1024], P(None, 'tp'), may hold values from -0.1875 to 0.1875
- key_weight: bfloat16 [2048, 256], replicated, may hold values from -0.1875 to 0.1875
- value_weight: bfloat16 [2048, 256], replicated, may hold values from -0.125 to 0.125
- out_weight: bfloat16 [1024, 2048], replicated, may hold values from -0.1875 to 0.1875
- head_gain: float32 [128], replicated, may hold values from 0.1 to 1.9
- lambdas: float32 [8], P('tp'), may hold values from 0.3 to 0.8
Outputs:
- mixed: bfloat16 [16384, 2048], P(('sp', 'tp'))
All inputs are finite; a program needn't handle non-finite values.
Results may differ from a plain program's by a relative error of at most 0.018.
The roundings to bfloat16 on the way count: a program that leaves them out, or rounds other values in their place, can miss the bound.
Values may be sent and summed in bfloat16 or wider, within the bound.
No kernel may reach another device: no remote copies, remote signals or barrier semaphores. Data moves between devices by JAX's collectives and lax.ppermute only.
A program may use at most 64 MiB of HBM per device.

v0:
```python
import jax
import jax.numpy as jnp
from jax import lax
from jax.sharding import PartitionSpec as P

H = 8
DH = 64
DV = 128


epsilon = 1e-06
rope_base = 10000.0
fold_span = 2048


def joined_along(parts, dim):
    parts = jnp.moveaxis(parts, 0, dim)
    shape = parts.shape
    return parts.reshape(*shape[:dim], shape[dim] * shape[dim + 1], *shape[dim + 2 :])


def copy_for_each(x, axis):
    count = lax.axis_size(axis)
    return lax.all_to_all(jnp.broadcast_to(x[None], (count, *x.shape)), axis, 0, 0, tiled=True)


def gather_directly(x, axis, dim):
    return joined_along(copy_for_each(x, axis), dim)


def sent_together(arrays, axis, dim, along):
    ends, at = ([], 0)
    for a in arrays[:-1]:
        at += a.shape[along]
        ends.append(at)
    both = jnp.concatenate(arrays, axis=along)
    return tuple(jnp.split(lax.all_gather(both, axis, axis=dim, tiled=True), ends, axis=along))


def rotate(tensor_in, places):
    head_dim = tensor_in.shape[-1]
    half_dim = head_dim // 2
    frequency = rope_base ** (-(jnp.arange(half_dim, dtype=jnp.float32) * 2.0) / head_dim)
    angles = places[:, None] * frequency[None, :]
    angles = angles.reshape((places.shape[0],) + (1,) * (tensor_in.ndim - 2) + (half_dim,))
    cosine = jnp.cos(angles)
    sine_part = jnp.sin(angles)
    first = tensor_in[..., :half_dim]
    second = tensor_in[..., half_dim:]
    return jnp.concatenate(
        [first * cosine - second * sine_part, first * sine_part + second * cosine], axis=-1
    )


def local(tokens, query_weight, key_weight, value_weight, out_weight, head_gain, lambdas):
    heads_dev = query_weight.shape[1] // (2 * DH)
    kv_heads = key_weight.shape[1] // (2 * DH)
    group_size = H // kv_heads
    kv_index = lax.axis_index("tp") * heads_dev // group_size
    key_cols = lax.dynamic_slice_in_dim(key_weight, kv_index * (2 * DH), 2 * DH, 1)
    value_cols = lax.dynamic_slice_in_dim(value_weight, kv_index * DV, DV, 1)
    stacked = jnp.concatenate([query_weight, key_cols, value_cols], axis=1)
    projected = jnp.dot(
        gather_directly(tokens, "tp", 0), stacked, preferred_element_type=jnp.float32
    )
    seq_rows = projected.shape[0]
    places = (lax.axis_index("sp") * seq_rows + jnp.arange(seq_rows, dtype=jnp.int32)).astype(
        jnp.float32
    )
    query_cols = heads_dev * 2 * DH
    queries = rotate(projected[:, :query_cols].reshape(seq_rows, heads_dev, 2, DH), places).astype(
        jnp.bfloat16
    )
    key_rows = rotate(
        projected[:, query_cols : query_cols + 2 * DH].reshape(seq_rows, 2, DH), places
    )
    key_rows = key_rows.astype(jnp.bfloat16).reshape(seq_rows, 2 * DH)
    value_rows = projected[:, query_cols + 2 * DH :].astype(jnp.bfloat16)
    score_scale = DH ** (-0.5)

    def update(carried, key_block, value_block):
        running_max, running_sum, weighted = carried
        scores = (
            jnp.einsum(
                "qhcd,kcd->cqhk",
                queries,
                key_block.reshape(key_block.shape[0], 2, DH),
                preferred_element_type=jnp.float32,
            )
            * score_scale
        )
        new_max = jnp.maximum(running_max, jnp.max(scores, axis=-1))
        weights = jnp.exp(scores - new_max[..., None])
        shrink = jnp.exp(running_max - new_max)
        running_sum = shrink * running_sum + jnp.sum(weights, axis=-1)
        weighted = shrink[..., None] * weighted + jnp.einsum(
            "cqhk,kv->cqhv",
            weights.astype(jnp.bfloat16),
            value_block,
            preferred_element_type=jnp.float32,
        )
        return (new_max, running_sum, weighted)

    initial = (
        jnp.full((2, seq_rows, heads_dev), -1e30, jnp.float32),
        jnp.zeros((2, seq_rows, heads_dev), jnp.float32),
        jnp.zeros((2, seq_rows, heads_dev, DV), jnp.float32),
    )
    key_piece, value_piece = sent_together((key_rows, value_rows), "sp", 0, 1)
    row_count = key_piece.shape[0]

    def one_span(state_now, span_index):
        key_block = lax.dynamic_slice_in_dim(key_piece, span_index * fold_span, fold_span, 0)
        value_block = lax.dynamic_slice_in_dim(value_piece, span_index * fold_span, fold_span, 0)
        return (update(state_now, key_block, value_block), None)

    running_max, running_sum, weighted = lax.scan(
        one_span, initial, jnp.arange(row_count // fold_span, dtype=jnp.int32)
    )[0]
    attended = (
        weighted[0] / running_sum[0][..., None]
        - lambdas[None, :, None] * weighted[1] / running_sum[1][..., None]
    )
    mean_square = jnp.mean(attended * attended, axis=-1, keepdims=True)
    normed = (attended * lax.rsqrt(mean_square + epsilon) * head_gain).astype(jnp.bfloat16)
    normed = normed.reshape(seq_rows, heads_dev * DV)
    regrouped = lax.all_to_all(normed, "tp", split_axis=0, concat_axis=1, tiled=True)
    return jnp.dot(regrouped, out_weight, preferred_element_type=jnp.float32).astype(jnp.bfloat16)


def solution(mesh):
    return jax.shard_map(
        local,
        mesh=mesh,
        in_specs=(P(("sp", "tp"), None), P(None, "tp"), P(), P(), P(), P(), P("tp")),
        out_specs=P(("sp", "tp"), None),
        check_vma=False,
    )
```

profile of v0, /device:TPU:1, one launch (start us, length us, event | category | flops | bytes accessed | tf_op | source)
XLA Modules:
  0.0 288.7 jit_solution(8956814849785031514)
XLA Ops:
  6.5 2.5 broadcast_in_dim.11
  9.1 6.7 %all-to-all-start = ((bf16[8,64,2048]{2,1,0:T(8,128)(2,1)}), bf16[8,64,2048]{2,1,0:T(8,128)(2,1)S(1)}, u32[]{:S(2)}, u32[]{:S(2)}) async-start(bf16[8,64,2048]{2,1,0:T(8,128)(2,1)} %broadcast_in_dim.11), calls=%async_computation | async-start | bytes 4194304 | tf_op jit(solution)/shard_map/all_to_all | solution.py:24
  17.4 24.6 %all-to-all-done = bf16[8,64,2048]{2,1,0:T(8,128)(2,1)S(1)} async-done(((bf16[8,64,2048]{2,1,0:T(8,128)(2,1)}), bf16[8,64,2048]{2,1,0:T(8,128)(2,1)S(1)}, u32[]{:S(2)}, u32[]{:S(2)}) %all-to-all-start) | async-done | bytes 2097184 | tf_op jit(solution)/shard_map/all_to_all | solution.py:24
  45.7 98.9 %all-gather.2.cloned.1.call-done = bf16[16384,256]{0,1:T(8,128)(2,1)} async-done(((bf16[512,256]{0,1:T(8,128)(2,1)}), bf16[16384,256]{0,1:T(8,128)(2,1)}) %all-gather.2.cloned.1.call-update) | async-done | bytes 8388624 | tf_op jit(solution)/shard_map/all_gather | solution.py:37
  144.6 5.8 %fusion.33 = (bf16[16384,128]{0,1:T(8,128)(2,1)}, bf16[16384,128]{0,1:T(8,128)(2,1)}) fusion(bf16[16384,256]{0,1:T(8,128)(2,1)} %all-gather.2.cloned.1.call-done), kind=kLoop, calls=%fused_computation.57 | loop fusion | bytes 16777216 | tf_op jit(solution)/shard_map/split | solution.py:37
  150.4 113.6 %while.15 = (s32[]{:T(128)}, f32[2,512,1]{1,0,2:T(2,128)S(1)}, f32[2,512,1]{1,0,2:T(2,128)S(1)}, f32[2,512,1,128]{3,1,0,2:T(8,128)S(1)}, s32[8]{0:T(128)S(1)}, /...) while((s32[]{:T(128)}, f32[2,512,1]{1,0,2:T(2,128)S(1)}, ...), condition=%wide.region_3.4_spmd.clone, body=%wide.region_0.3_spmd.clone.sunk | while | flops 822482944 | bytes 62062812 | solution.py:117
  152.8 4.5 %bitcast_reduce_fusion.2 = (f32[2,512]{1,0:T(2,128)S(1)}, f32[2,2048,512]{2,1,0:T(8,128)}) fusion(bf16[2048,2,64]{0,2,1:T(8,128)(2,1)S(1)} %bitcast.99, bf16[512,1,2,64]{0,3,2,1:T(8,128)(2,1)S(1)} %get-tuple-element.234), kind=kOutput, calls=%fused_computation.1.clone.1 | convolution fusion | flops 272628736 | bytes 9048064 | tf_op jit(solution)/shard_map/while/body/eval_jaxpr/qhcd,kcd->cqhk/dot_general | solution.py:84
  157.3 5.3 %fusion.50 = f32[2,512,1,128]{3,1,0,2:T(8,128)S(1)} fusion(f32[2,2048,512]{2,1,0:T(8,128)} %get-tuple-element.202, f32[2,512]{1,0:T(2,128)S(1)} %bitcast.102, f32[2,512,1,128]{3,1,0,2:T(8,128)S(1)} %get-tuple-element.219, bf16[16384,128]{0,1:T(8,128)(2,1)} %get-tuple-element.235, s32[]{:T(128)S(6)} %select_n.17, ...), kind=kOutput, calls=%fused_computation.7.clone.1 | convolution fusion | flops 543555584 | bytes 9969669 | tf_op jit(solution)/shard_map/while/body/eval_jaxpr/cqhk,kv->cqhv/dot_general | solution.py:96
  167.0 4.5 %bitcast_reduce_fusion.2 = (f32[2,512]{1,0:T(2,128)S(1)}, f32[2,2048,512]{2,1,0:T(8,128)}) fusion(bf16[2048,2,64]{0,2,1:T(8,128)(2,1)S(1)} %bitcast.99, bf16[512,1,2,64]{0,3,2,1:T(8,128)(2,1)S(1)} %get-tuple-element.234), kind=kOutput, calls=%fused_computation.1.clone.1 | convolution fusion | flops 272628736 | bytes 9048064 | tf_op jit(solution)/shard_map/while/body/eval_jaxpr/qhcd,kcd->cqhk/dot_general | solution.py:84
  171.5 5.3 %fusion.50 = f32[2,512,1,128]{3,1,0,2:T(8,128)S(1)} fusion(f32[2,2048,512]{2,1,0:T(8,128)} %get-tuple-element.202, f32[2,512]{1,0:T(2,128)S(1)} %bitcast.102, f32[2,512,1,128]{3,1,0,2:T(8,128)S(1)} %get-tuple-element.219, bf16[16384,128]{0,1:T(8,128)(2,1)} %get-tuple-element.235, s32[]{:T(128)S(6)} %select_n.17, ...), kind=kOutput, calls=%fused_computation.7.clone.1 | convolution fusion | flops 543555584 | bytes 9969669 | tf_op jit(solution)/shard_map/while/body/eval_jaxpr/cqhk,kv->cqhv/dot_general | solution.py:96
  181.2 4.5 %bitcast_reduce_fusion.2 = (f32[2,512]{1,0:T(2,128)S(1)}, f32[2,2048,512]{2,1,0:T(8,128)}) fusion(bf16[2048,2,64]{0,2,1:T(8,128)(2,1)S(1)} %bitcast.99, bf16[512,1,2,64]{0,3,2,1:T(8,128)(2,1)S(1)} %get-tuple-element.234), kind=kOutput, calls=%fused_computation.1.clone.1 | convolution fusion | flops 272628736 | bytes 9048064 | tf_op jit(solution)/shard_map/while/body/eval_jaxpr/qhcd,kcd->cqhk/dot_general | solution.py:84
  185.7 5.3 %fusion.50 = f32[2,512,1,128]{3,1,0,2:T(8,128)S(1)} fusion(f32[2,2048,512]{2,1,0:T(8,128)} %get-tuple-element.202, f32[2,512]{1,0:T(2,128)S(1)} %bitcast.102, f32[2,512,1,128]{3,1,0,2:T(8,128)S(1)} %get-tuple-element.219, bf16[16384,128]{0,1:T(8,128)(2,1)} %get-tuple-element.235, s32[]{:T(128)S(6)} %select_n.17, ...), kind=kOutput, calls=%fused_computation.7.clone.1 | convolution fusion | flops 543555584 | bytes 9969669 | tf_op jit(solution)/shard_map/while/body/eval_jaxpr/cqhk,kv->cqhv/dot_general | solution.py:96
  195.4 4.5 %bitcast_reduce_fusion.2 = (f32[2,512]{1,0:T(2,128)S(1)}, f32[2,2048,512]{2,1,0:T(8,128)}) fusion(bf16[2048,2,64]{0,2,1:T(8,128)(2,1)S(1)} %bitcast.99, bf16[512,1,2,64]{0,3,2,1:T(8,128)(2,1)S(1)} %get-tuple-element.234), kind=kOutput, calls=%fused_computation.1.clone.1 | convolution fusion | flops 272628736 | bytes 9048064 | tf_op jit(solution)/shard_map/while/body/eval_jaxpr/qhcd,kcd->cqhk/dot_general | solution.py:84
  199.9 5.3 %fusion.50 = f32[2,512,1,128]{3,1,0,2:T(8,128)S(1)} fusion(f32[2,2048,512]{2,1,0:T(8,128)} %get-tuple-element.202, f32[2,512]{1,0:T(2,128)S(1)} %bitcast.102, f32[2,512,1,128]{3,1,0,2:T(8,128)S(1)} %get-tuple-element.219, bf16[16384,128]{0,1:T(8,128)(2,1)} %get-tuple-element.235, s32[]{:T(128)S(6)} %select_n.17, ...), kind=kOutput, calls=%fused_computation.7.clone.1 | convolution fusion | flops 543555584 | bytes 9969669 | tf_op jit(solution)/shard_map/while/body/eval_jaxpr/cqhk,kv->cqhv/dot_general | solution.py:96
  209.6 4.5 %bitcast_reduce_fusion.2 = (f32[2,512]{1,0:T(2,128)S(1)}, f32[2,2048,512]{2,1,0:T(8,128)}) fusion(bf16[2048,2,64]{0,2,1:T(8,128)(2,1)S(1)} %bitcast.99, bf16[512,1,2,64]{0,3,2,1:T(8,128)(2,1)S(1)} %get-tuple-element.234), kind=kOutput, calls=%fused_computation.1.clone.1 | convolution fusion | flops 272628736 | bytes 9048064 | tf_op jit(solution)/shard_map/while/body/eval_jaxpr/qhcd,kcd->cqhk/dot_general | solution.py:84
  214.1 5.3 %fusion.50 = f32[2,512,1,128]{3,1,0,2:T(8,128)S(1)} fusion(f32[2,2048,512]{2,1,0:T(8,128)} %get-tuple-element.202, f32[2,512]{1,0:T(2,128)S(1)} %bitcast.102, f32[2,512,1,128]{3,1,0,2:T(8,128)S(1)} %get-tuple-element.219, bf16[16384,128]{0,1:T(8,128)(2,1)} %get-tuple-element.235, s32[]{:T(128)S(6)} %select_n.17, ...), kind=kOutput, calls=%fused_computation.7.clone.1 | convolution fusion | flops 543555584 | bytes 9969669 | tf_op jit(solution)/shard_map/while/body/eval_jaxpr/cqhk,kv->cqhv/dot_general | solution.py:96
  223.8 4.5 %bitcast_reduce_fusion.2 = (f32[2,512]{1,0:T(2,128)S(1)}, f32[2,2048,512]{2,1,0:T(8,128)}) fusion(bf16[2048,2,64]{0,2,1:T(8,128)(2,1)S(1)} %bitcast.99, bf16[512,1,2,64]{0,3,2,1:T(8,128)(2,1)S(1)} %get-tuple-element.234), kind=kOutput, calls=%fused_computation.1.clone.1 | convolution fusion | flops 272628736 | bytes 9048064 | tf_op jit(solution)/shard_map/while/body/eval_jaxpr/qhcd,kcd->cqhk/dot_general | solution.py:84
  228.3 5.3 %fusion.50 = f32[2,512,1,128]{3,1,0,2:T(8,128)S(1)} fusion(f32[2,2048,512]{2,1,0:T(8,128)} %get-tuple-element.202, f32[2,512]{1,0:T(2,128)S(1)} %bitcast.102, f32[2,512,1,128]{3,1,0,2:T(8,128)S(1)} %get-tuple-element.219, bf16[16384,128]{0,1:T(8,128)(2,1)} %get-tuple-element.235, s32[]{:T(128)S(6)} %select_n.17, ...), kind=kOutput, calls=%fused_computation.7.clone.1 | convolution fusion | flops 543555584 | bytes 9969669 | tf_op jit(solution)/shard_map/while/body/eval_jaxpr/cqhk,kv->cqhv/dot_general | solution.py:96
  238.0 4.5 %bitcast_reduce_fusion.2 = (f32[2,512]{1,0:T(2,128)S(1)}, f32[2,2048,512]{2,1,0:T(8,128)}) fusion(bf16[2048,2,64]{0,2,1:T(8,128)(2,1)S(1)} %bitcast.99, bf16[512,1,2,64]{0,3,2,1:T(8,128)(2,1)S(1)} %get-tuple-element.234), kind=kOutput, calls=%fused_computation.1.clone.1 | convolution fusion | flops 272628736 | bytes 9048064 | tf_op jit(solution)/shard_map/while/body/eval_jaxpr/qhcd,kcd->cqhk/dot_general | solution.py:84
  242.5 5.3 %fusion.50 = f32[2,512,1,128]{3,1,0,2:T(8,128)S(1)} fusion(f32[2,2048,512]{2,1,0:T(8,128)} %get-tuple-element.202, f32[2,512]{1,0:T(2,128)S(1)} %bitcast.102, f32[2,512,1,128]{3,1,0,2:T(8,128)S(1)} %get-tuple-element.219, bf16[16384,128]{0,1:T(8,128)(2,1)} %get-tuple-element.235, s32[]{:T(128)S(6)} %select_n.17, ...), kind=kOutput, calls=%fused_computation.7.clone.1 | convolution fusion | flops 543555584 | bytes 9969669 | tf_op jit(solution)/shard_map/while/body/eval_jaxpr/cqhk,kv->cqhv/dot_general | solution.py:96
  252.2 4.5 %bitcast_reduce_fusion.2 = (f32[2,512]{1,0:T(2,128)S(1)}, f32[2,2048,512]{2,1,0:T(8,128)}) fusion(bf16[2048,2,64]{0,2,1:T(8,128)(2,1)S(1)} %bitcast.99, bf16[512,1,2,64]{0,3,2,1:T(8,128)(2,1)S(1)} %get-tuple-element.234), kind=kOutput, calls=%fused_computation.1.clone.1 | convolution fusion | flops 272628736 | bytes 9048064 | tf_op jit(solution)/shard_map/while/body/eval_jaxpr/qhcd,kcd->cqhk/dot_general | solution.py:84
  256.7 5.3 %fusion.50 = f32[2,512,1,128]{3,1,0,2:T(8,128)S(1)} fusion(f32[2,2048,512]{2,1,0:T(8,128)} %get-tuple-element.202, f32[2,512]{1,0:T(2,128)S(1)} %bitcast.102, f32[2,512,1,128]{3,1,0,2:T(8,128)S(1)} %get-tuple-element.219, bf16[16384,128]{0,1:T(8,128)(2,1)} %get-tuple-element.235, s32[]{:T(128)S(6)} %select_n.17, ...), kind=kOutput, calls=%fused_computation.7.clone.1 | convolution fusion | flops 543555584 | bytes 9969669 | tf_op jit(solution)/shard_map/while/body/eval_jaxpr/cqhk,kv->cqhv/dot_general | solution.py:96
  264.9 13.2 %all_to_all.21 = bf16[8,64,128]{2,1,0:T(8,128)(2,1)S(1)} all-to-all(bf16[8,64,128]{2,1,0:T(8,128)(2,1)S(1)} %multiply_convert_fusion), channel_id=1, replica_groups=mesh['sp'=32,'tp'=8] {'tp'}, dimensions={0} | all-to-all | bytes 262144 | tf_op jit(solution)/shard_map/all_to_all | solution.py:127
  278.1 3.7 %convolution_convert_fusion = bf16[64,2048]{1,0:T(8,128)(2,1)} fusion(bf16[1024,2048]{1,0:T(8,128)(2,1)} %param.13, bf16[8,64,128]{2,1,0:T(8,128)(2,1)S(1)} %all_to_all.21), kind=kOutput, calls=%fused_computation.22 | convolution fusion | flops 268566528 | bytes 4587520 | tf_op jit(solution)/shard_map/dot_general | solution.py:128
  (92 shorter events, 35.2 us)
Async XLA Ops:
  9.1 32.9 %all-to-all-start = ((bf16[8,64,2048]{2,1,0:T(8,128)(2,1)}), bf16[8,64,2048]{2,1,0:T(8,128)(2,1)S(1)}, u32[]{:S(2)}, u32[]{:S(2)}) async-start(bf16[8,64,2048]{2,1,0:T(8,128)(2,1)} %broadcast_in_dim.11), calls=%async_computation | async-start | bytes 4194304 | tf_op jit(solution)/shard_map/all_to_all | solution.py:24
  15.8 128.8 %all-gather.2.cloned.1.call-start = ((), (), s32[]{:S(2)}) async-start(), calls=%async_computation.2 | async-start | bytes 8650752 | tf_op jit(solution)/shard_map/all_gather | solution.py:37
  150.4 114.2 %copy-start.1 = (f32[128]{0:T(128)S(1)}, f32[128]{0:T(128)}, u32[]{:S(2)}) copy-start(f32[128]{0:T(128)} %param.14) | copy-start | bytes 1540
  157.3 5.9 %copy-start = (f32[2,2048,512]{2,1,0:T(8,128)S(1)}, f32[2,2048,512]{2,1,0:T(8,128)}, u32[]{:S(2)}) copy-start(f32[2,2048,512]{2,1,0:T(8,128)} %get-tuple-element.202) | copy-start | bytes 25165828 | tf_op jit(solution)/shard_map/while
  171.5 5.9 %copy-start = (f32[2,2048,512]{2,1,0:T(8,128)S(1)}, f32[2,2048,512]{2,1,0:T(8,128)}, u32[]{:S(2)}) copy-start(f32[2,2048,512]{2,1,0:T(8,128)} %get-tuple-element.202) | copy-start | bytes 25165828 | tf_op jit(solution)/shard_map/while
  185.7 5.9 %copy-start = (f32[2,2048,512]{2,1,0:T(8,128)S(1)}, f32[2,2048,512]{2,1,0:T(8,128)}, u32[]{:S(2)}) copy-start(f32[2,2048,512]{2,1,0:T(8,128)} %get-tuple-element.202) | copy-start | bytes 25165828 | tf_op jit(solution)/shard_map/while
  199.9 5.9 %copy-start = (f32[2,2048,512]{2,1,0:T(8,128)S(1)}, f32[2,2048,512]{2,1,0:T(8,128)}, u32[]{:S(2)}) copy-start(f32[2,2048,512]{2,1,0:T(8,128)} %get-tuple-element.202) | copy-start | bytes 25165828 | tf_op jit(solution)/shard_map/while
  214.1 5.9 %copy-start = (f32[2,2048,512]{2,1,0:T(8,128)S(1)}, f32[2,2048,512]{2,1,0:T(8,128)}, u32[]{:S(2)}) copy-start(f32[2,2048,512]{2,1,0:T(8,128)} %get-tuple-element.202) | copy-start | bytes 25165828 | tf_op jit(solution)/shard_map/while
  228.3 5.9 %copy-start = (f32[2,2048,512]{2,1,0:T(8,128)S(1)}, f32[2,2048,512]{2,1,0:T(8,128)}, u32[]{:S(2)}) copy-start(f32[2,2048,512]{2,1,0:T(8,128)} %get-tuple-element.202) | copy-start | bytes 25165828 | tf_op jit(solution)/shard_map/while
  242.5 5.9 %copy-start = (f32[2,2048,512]{2,1,0:T(8,128)S(1)}, f32[2,2048,512]{2,1,0:T(8,128)}, u32[]{:S(2)}) copy-start(f32[2,2048,512]{2,1,0:T(8,128)} %get-tuple-element.202) | copy-start | bytes 25165828 | tf_op jit(solution)/shard_map/while
  256.7 5.9 %copy-start = (f32[2,2048,512]{2,1,0:T(8,128)S(1)}, f32[2,2048,512]{2,1,0:T(8,128)}, u32[]{:S(2)}) copy-start(f32[2,2048,512]{2,1,0:T(8,128)} %get-tuple-element.202) | copy-start | bytes 25165828 | tf_op jit(solution)/shard_map/while
Sparse Core Ops, SparseCore 0:
  45.1 99.4 all-gather.1
where the time goes:
time: 289 us
  waiting for transfers between devices  124 us (43%)
  matrix products  84.1 us (29%)
  local copies, waits for them, and re-layouts  28.4 us (10%)
  between operations  14.2 us (5%)
  blocking collectives  13.2 us (5%)
  other arithmetic  13 us (4%)
  starting transfers between devices  6.71 us (2%)
  loops' own time  5.6 us (2%)
    all_gather x1, waiting for transfers between devices, sent_together(): lax.all_gather(both, axis, axis=dim, tiled=True)  98.9 us
    dot_general x8, matrix products, update(): jnp.einsum('cqhk,kv->cqhv', weights.astype(jnp.bfloat16), value_block, pr...  42.1 us
    dot_general x8, matrix products, update(): jnp.einsum('qhcd,kcd->cqhk', queries, key_block.reshape(key_block.shape[0...  36.1 us
    all_to_all x1, waiting for transfers between devices, copy_for_each(): lax.all_to_all(jnp.broadcast_to(x[None], (count, *x.shape)), axis, 0, 0,...  24.6 us
    all_to_all x1, blocking collectives, local(): lax.all_to_all(normed, 'tp', split_axis=0, concat_axis=1, tiled=True)  13.2 us
    reduce_sum x8, other arithmetic, update(): running_sum = shrink * running_sum + jnp.sum(weights, axis=-1)  11 us
    dynamic_slice x8, local copies, waits for them, and re-layouts, one_span(): lax.dynamic_slice_in_dim(key_piece, span_index * fold_span, fold_span, 0)  8.65 us
    all_to_all x1, starting transfers between devices, copy_for_each(): lax.all_to_all(jnp.broadcast_to(x[None], (count, *x.shape)), axis, 0, 0,...  6.7 us
  transfers between devices with their start and end apart: 2, of which 2 were waited for; matrix products, arithmetic and copies ran while one was open for 1% of the time, Pallas kernels for 0%

commit v1 on v0

--- a/solution.py
+++ b/solution.py
@@ -1,3 +1,6 @@
+import math, functools
+from jax.experimental import pallas as pl
+from jax.experimental.pallas import tpu as pltpu
 import jax
 import jax.numpy as jnp
 from jax import lax
@@ -52,6 +55,62 @@
     )
 
 
+EXP_SCALE = math.log2(math.e) * 64 ** -0.5
+ACC_ROWS = 136
+
+def fold_block(q_ref, kv_ref, m_ref, acc_ref, start, kb, cb):
+    n = q_ref.shape[1]
+    k = kv_ref[pl.ds(start, kb), 0:128]
+    v = kv_ref[pl.ds(start, kb), 128:256]
+    vt = jnp.concatenate([v.T, jnp.ones((ACC_ROWS - 128, kb), jnp.bfloat16)], axis=0)
+    def score(j):
+        return jnp.dot(k, q_ref[:, j * cb:(j + 1) * cb], preferred_element_type=jnp.float32)
+    nxt = score(0)
+    nt = n // cb
+    for j in range(nt):
+        s = nxt
+        if j + 1 < nt:
+            nxt = score(j + 1)
+        cols = slice(j * cb, (j + 1) * cb)
+        old = m_ref[0:1, cols]
+        new = jnp.maximum(old, jnp.max(s, axis=0, keepdims=True))
+        m_ref[0:1, cols] = new
+        p = jnp.exp2(s * EXP_SCALE - new * EXP_SCALE).astype(jnp.bfloat16)
+        alpha = jnp.exp2((old - new) * EXP_SCALE)
+        acc_ref[:, cols] = acc_ref[:, cols] * alpha + jnp.dot(vt, p, preferred_element_type=jnp.float32)
+
+def attn_kernel(*refs, nkv, first, kb, cb):
+    q_ref = refs[0]
+    kvs = refs[1:1 + nkv]
+    m_ref, acc_ref = refs[-2:]
+    if first:
+        m_ref[...] = jnp.full(m_ref.shape, -3e38, jnp.float32)
+        acc_ref[...] = jnp.zeros(acc_ref.shape, jnp.float32)
+    else:
+        m_ref[...] = refs[1 + nkv][...]
+        acc_ref[...] = refs[2 + nkv][...]
+    for kv_ref in kvs:
+        steps = kv_ref.shape[0] // kb
+        def body(i, _):
+            fold_block(q_ref, kv_ref, m_ref, acc_ref, pl.multiple_of(i * kb, kb), kb, cb)
+            return 0
+        lax.fori_loop(0, steps, body, 0)
+
+def attn(q, kvs, carry=None, kb=1024, cb=512):
+    n = q.shape[1]
+    nk = sum(a.shape[0] for a in kvs)
+    vm = pl.BlockSpec(memory_space=pltpu.VMEM)
+    ops = [q, *kvs] + ([] if carry is None else list(carry))
+    al = {} if carry is None else {len(ops) - 2: 0, len(ops) - 1: 1}
+    return pl.pallas_call(
+        functools.partial(attn_kernel, nkv=len(kvs), first=carry is None, kb=kb, cb=cb),
+        out_shape=(jax.ShapeDtypeStruct((8, n), jnp.float32), jax.ShapeDtypeStruct((ACC_ROWS, n), jnp.float32)),
+        in_specs=[vm] * len(ops), out_specs=(vm, vm), input_output_aliases=al,
+        cost_estimate=pl.CostEstimate(flops=2 * nk * n * 256, transcendentals=nk * n, bytes_accessed=nk * 512),
+        compiler_params=pltpu.CompilerParams(vmem_limit_bytes=56 * 2**20),
+    )(*ops)
+
+
 def local(tokens, query_weight, key_weight, value_weight, out_weight, head_gain, lambdas):
     heads_dev = query_weight.shape[1] // (2 * DH)
     kv_heads = key_weight.shape[1] // (2 * DH)
@@ -76,51 +135,19 @@
     )
     key_rows = key_rows.astype(jnp.bfloat16).reshape(seq_rows, 2 * DH)
     value_rows = projected[:, query_cols + 2 * DH :].astype(jnp.bfloat16)
-    score_scale = DH ** (-0.5)
-
-    def update(carried, key_block, value_block):
-        running_max, running_sum, weighted = carried
-        scores = (
-            jnp.einsum(
-                "qhcd,kcd->cqhk",
-                queries,
-                key_block.reshape(key_block.shape[0], 2, DH),
-                preferred_element_type=jnp.float32,
-            )
-            * score_scale
-        )
-        new_max = jnp.maximum(running_max, jnp.max(scores, axis=-1))
-        weights = jnp.exp(scores - new_max[..., None])
-        shrink = jnp.exp(running_max - new_max)
-        running_sum = shrink * running_sum + jnp.sum(weights, axis=-1)
-        weighted = shrink[..., None] * weighted + jnp.einsum(
-            "cqhk,kv->cqhv",
-            weights.astype(jnp.bfloat16),
-            value_block,
-            preferred_element_type=jnp.float32,
-        )
-        return (new_max, running_sum, weighted)
-
-    initial = (
-        jnp.full((2, seq_rows, heads_dev), -1e30, jnp.float32),
-        jnp.zeros((2, seq_rows, heads_dev), jnp.float32),
-        jnp.zeros((2, seq_rows, heads_dev, DV), jnp.float32),
+    blank = jnp.zeros((DH, seq_rows * heads_dev), jnp.bfloat16)
+    first_map = queries[:, :, 0].reshape(seq_rows * heads_dev, DH).T
+    second_map = queries[:, :, 1].reshape(seq_rows * heads_dev, DH).T
+    columns = jnp.concatenate(
+        [jnp.concatenate([first_map, blank], 0), jnp.concatenate([blank, second_map], 0)], 1
     )
-    key_piece, value_piece = sent_together((key_rows, value_rows), "sp", 0, 1)
-    row_count = key_piece.shape[0]
-
-    def one_span(state_now, span_index):
-        key_block = lax.dynamic_slice_in_dim(key_piece, span_index * fold_span, fold_span, 0)
-        value_block = lax.dynamic_slice_in_dim(value_piece, span_index * fold_span, fold_span, 0)
-        return (update(state_now, key_block, value_block), None)
-
-    running_max, running_sum, weighted = lax.scan(
-        one_span, initial, jnp.arange(row_count // fold_span, dtype=jnp.int32)
-    )[0]
-    attended = (
-        weighted[0] / running_sum[0][..., None]
-        - lambdas[None, :, None] * weighted[1] / running_sum[1][..., None]
+    gathered = lax.all_gather(
+        jnp.concatenate([key_rows, value_rows], 1), "sp", axis=0, tiled=True
     )
+    _, folded = attn(columns, [gathered])
+    folded = folded.reshape(ACC_ROWS, 2, seq_rows, heads_dev)
+    each = jnp.moveaxis(folded[:DV], 0, -1) / folded[DV][..., None]
+    attended = each[0] - lambdas[None, :, None] * each[1]
     mean_square = jnp.mean(attended * attended, axis=-1, keepdims=True)
     normed = (attended * lax.rsqrt(mean_square + epsilon) * head_gain).astype(jnp.bfloat16)
     normed = normed.reshape(seq_rows, heads_dev * DV)

time: 289 us -> 199 us (0.69)
  matrix products: 84.1 us -> 6.02 us
  Pallas kernels: 0 us -> 31.9 us
  local copies, waits for them, and re-layouts: 28.4 us -> 6.39 us
  other arithmetic: 13 us -> 2.41 us
  loops' own time: 5.6 us -> 0 us
  waiting for transfers between devices: 124 us -> 121 us
    dot_general x16 -> x0, matrix products: 78.3 us -> none  [the longest x8 42.1 us: update(): jnp.einsum('cqhk,kv->cqhv', weights.astype(jnp.bfloat16), value_block, pr...]
    pallas_call x0 -> x1, Pallas kernels: none -> 31.9 us  [attn(): pl.pallas_call(functools.partial(attn_kernel, nkv=len(kvs), first=carry i...]
    dynamic_slice x16 -> x0, local copies, waits for them, and re-layouts: 13.3 us -> none  [the longest x8 8.65 us: one_span(): lax.dynamic_slice_in_dim(key_piece, span_index * fold_span, fold_span, 0)]
    reduce_sum x8 -> x0, other arithmetic: 11 us -> none  [update(): running_sum = shrink * running_sum + jnp.sum(weights, axis=-1)]
    split x1 -> x0, local copies, waits for them, and re-layouts: 5.79 us -> none  [sent_together(): jnp.split(lax.all_gather(both, axis, axis=dim, tiled=True), ends, axis=al...]
    another operation x1 -> x0, loops' own time: 5.6 us -> none  [local(): lax.scan(one_span, initial, jnp.arange(row_count // fold_span, dtype=jnp....]
    while x24 -> x0, local copies, waits for them, and re-layouts: 5.16 us -> none
where the time goes in v1:
time: 199 us
  waiting for transfers between devices  121 us (61%)
  Pallas kernels  31.9 us (16%)
  between operations  14.2 us (7%)
  blocking collectives  10.6 us (5%)
  starting transfers between devices  6.71 us (3%)
  local copies, waits for them, and re-layouts  6.39 us (3%)
  matrix products  6.02 us (3%)
  other arithmetic  2.41 us (1%)
    all_gather x1, waiting for transfers between devices, local(): lax.all_gather(jnp.concatenate([key_rows, value_rows], 1), 'sp', axis=0,...  96.1 us
    pallas_call x1, Pallas kernels, attn(): pl.pallas_call(functools.partial(attn_kernel, nkv=len(kvs), first=carry i...  31.9 us
    all_to_all x1, waiting for transfers between devices, copy_for_each(): lax.all_to_all(jnp.broadcast_to(x[None], (count, *x.shape)), axis, 0, 0,...  24.6 us
    all_to_all x1, blocking collectives, local(): lax.all_to_all(normed, 'tp', split_axis=0, concat_axis=1, tiled=True)  10.6 us
    all_to_all x1, starting transfers between devices, copy_for_each(): lax.all_to_all(jnp.broadcast_to(x[None], (count, *x.shape)), axis, 0, 0,...  6.7 us
  transfers between devices with their start and end apart: 2, of which 2 were waited for; matrix products, arithmetic and copies ran while one was open for 1% of the time, Pallas kernels for 0%

profile of v1, /device:TPU:1, one launch (start us, length us, event | category | flops | bytes accessed | tf_op | source)
XLA Modules:
  0.0 198.9 jit_solution(499710190722961290)
XLA Ops:
  6.5 2.5 %broadcast_in_dim.2 = bf16[8,64,2048]{2,1,0:T(8,128)(2,1)} broadcast(bf16[64,2048]{1,0:T(8,128)(2,1)} %param.7), dimensions={1,2} | broadcast | bytes 2359296 | tf_op jit(solution)/shard_map/broadcast_in_dim | solution.py:27
  9.1 6.7 %all-to-all-start = ((bf16[8,64,2048]{2,1,0:T(8,128)(2,1)}), bf16[8,64,2048]{2,1,0:T(8,128)(2,1)S(1)}, u32[]{:S(2)}, u32[]{:S(2)}) async-start(bf16[8,64,2048]{2,1,0:T(8,128)(2,1)} %broadcast_in_dim.2), calls=%async_computation | async-start | bytes 4194304 | tf_op jit(solution)/shard_map/all_to_all | solution.py:27
  15.8 0.0 all-gather.2.cloned.1.call-start
  15.8 0.3 multiply_cosine_fusion
  16.1 1.3 constant_dynamic-slice_fusion
  17.4 24.6 %all-to-all-done = bf16[8,64,2048]{2,1,0:T(8,128)(2,1)S(1)} async-done(((bf16[8,64,2048]{2,1,0:T(8,128)(2,1)}), bf16[8,64,2048]{2,1,0:T(8,128)(2,1)S(1)}, u32[]{:S(2)}, u32[]{:S(2)}) %all-to-all-start) | async-done | bytes 2097184 | tf_op jit(solution)/shard_map/all_to_all | solution.py:27
  42.0 2.3 %fusion.6 = f32[512,384]{1,0:T(8,128)S(1)} fusion(bf16[512,2048]{1,0:T(8,128)(2,1)S(1)} %bitcast.30, bf16[2048,128]{1,0:T(8,128)(2,1)S(1)} %get-tuple-element.19, bf16[2048,128]{1,0:T(8,128)(2,1)S(1)} %get-tuple-element.20, bf16[2048,128]{1,0:T(8,128)(2,1)} %param.8), kind=kOutput, calls=%fused_computation.7 | convolution fusion | flops 810024960 | bytes 4456448 | tf_op jit(solution)/shard_map/dot_general | solution.py:122
  44.4 0.1 copy.15
  44.6 0.1 copy.16
  44.7 0.8 pad_maximum_fusion
  45.5 0.0 all-gather.2.cloned.1.call-update
  46.1 0.1 copy.14
  46.3 0.7 fusion.11.refs_0_
  47.1 96.1 %all-gather.2.cloned.1.call-done.refs_1_ = bf16[16384,256]{1,0:T(8,128)(2,1)} async-done(((bf16[512,256]{1,0:T(8,128)(2,1)}), bf16[16384,256]{1,0:T(8,128)(2,1)}) %all-gather.2.cloned.1.call-update) | async-done | bytes 8388624 | tf_op jit(solution)/shard_map/all_gather | solution.py:144
  143.2 31.9 %shard_map.73 = (f32[8,1024]{1,0:T(8,128)}, f32[136,1024]{1,0:T(8,128)}) custom-call(bf16[128,1024]{1,0:T(8,128)(2,1)} %fusion.11.refs_0_, bf16[16384,256]{1,0:T(8,128)(2,1)} %all-gather.2.cloned.1.call-done.refs_1_), custom_call_target="tpu_custom_call" | custom-call | flops 8589934592 | bytes 8388608 | tf_op jit(solution)/shard_map/pallas_call | solution.py:105
  175.1 1.1 slice.53
  176.2 0.8 slice_reduce_fusion
  176.9 0.2 copy.20
  177.2 0.2 divide_bitcast_fusion
  177.4 0.1 multiply_reduce_fusion
  177.5 0.1 rsqrt.12
  177.6 0.1 multiply_convert_fusion
  177.8 10.6 %all_to_all.21 = bf16[8,64,128]{2,1,0:T(8,128)(2,1)S(1)} all-to-all(bf16[8,64,128]{2,1,0:T(8,128)(2,1)S(1)} %multiply_convert_fusion), channel_id=1, replica_groups=mesh['sp'=32,'tp'=8] {'tp'}, dimensions={0} | all-to-all | bytes 262144 | tf_op jit(solution)/shard_map/all_to_all | solution.py:154
  188.3 3.7 %convolution_convert_fusion = bf16[64,2048]{1,0:T(8,128)(2,1)} fusion(bf16[1024,2048]{1,0:T(8,128)(2,1)} %param.11, bf16[8,64,128]{2,1,0:T(8,128)(2,1)S(1)} %all_to_all.21), kind=kOutput, calls=%fused_computation | convolution fusion | flops 268566528 | bytes 4587520 | tf_op jit(solution)/shard_map/dot_general | solution.py:155
  (12 shorter events, 0.2 us)
Async XLA Ops:
  9.1 32.9 %all-to-all-start = ((bf16[8,64,2048]{2,1,0:T(8,128)(2,1)}), bf16[8,64,2048]{2,1,0:T(8,128)(2,1)S(1)}, u32[]{:S(2)}, u32[]{:S(2)}) async-start(bf16[8,64,2048]{2,1,0:T(8,128)(2,1)} %broadcast_in_dim.2), calls=%async_computation | async-start | bytes 4194304 | tf_op jit(solution)/shard_map/all_to_all | solution.py:27
  15.8 127.4 %all-gather.2.cloned.1.call-start = ((), (), s32[]{:S(2)}) async-start(), calls=%async_computation.2 | async-start | bytes 8650752 | tf_op jit(solution)/shard_map/all_gather | solution.py:144
  175.1 2.5 %copy-start = (f32[128]{0:T(128)S(1)}, f32[128]{0:T(128)}, u32[]{:S(2)}) copy-start(f32[128]{0:T(128)} %param.12) | copy-start | bytes 1540
Sparse Core Ops, SparseCore 0:
  45.6 97.5 all-gather.1
